TPU v7x, 32 devices: a whole 2x2x4 slice. The times are simulated.
32 devices in a mesh: ep: 4 (over y, x), tp: 8 (over z, core).
Axes of the slice: x: 2, y: 2, z: 4, core: 2. Of those that a mesh axis runs over, the one named last changes fastest.
Arguments:
- queries: bfloat16 [16, 64, 2, 512], P('tp', None, None, 'ep'), may hold values from -24 to 24
- key_vectors: bfloat16 [16, 64, 2, 512], P('tp', None, None, 'ep'), may hold values from -24 to 24
- value_vectors: bfloat16 [16, 64, 2, 512], P('tp', None, None, 'ep'), may hold values from -6 to 6
- mixer_weight: bfloat16 [1024, 2048], replicated, may hold values from -0.375 to 0.375
- expert_rows: bfloat16 [512, 2048], P('ep'), may hold values from -6 to 6
- norm_gain: float32 [2048], replicated, may hold values from 0.1 to 1.9
- route_ids: int32 [512, 2], P('ep'), may hold values from 0 to 7, all different within a row; in each aligned block of 128 rows (0 to 127, 128 to 255, ...) at most 64 rows name the same one
- route_logits: float32 [512, 2], P('ep'), may hold values from -4 to 4
- gate_weight: bfloat16 [8, 2048, 4096], P('ep', None, 'tp'), may hold values from -0.39648438 to 0.39648438
- up_weight: bfloat16 [8, 2048, 4096], P('ep', None, 'tp'), may hold values from -0.39648438 to 0.39648438
- down_weight: bfloat16 [8, 4096, 2048], P('ep', 'tp'), may hold values from -0.028076172 to 0.028076172
Outputs:
- mixer_out: bfloat16 [2, 512, 2048], P(None, ('ep', 'tp'))
- routed_out: bfloat16 [2048, 512], P('tp', 'ep')
Inputs may be any that keep to these rules, and one draw needn't show every extreme that they name: `route_ids`: each row names 2 different experts. Among the 128 rows of one index of ep no expert is named more than 64 times, a bound that some expert reaches in such a block.
All inputs are finite; a program needn't handle non-finite values.
Results may differ from a plain program's by a relative error of at most 0.018.
Values may be sent and summed in bfloat16 or wider, within the bound.
A program may use at most 64 MiB of HBM per device.

v0:
```python
import functools

import jax
import jax.numpy as jnp
from jax import lax
from jax.experimental import pallas as pl
from jax.experimental.pallas import tpu as pltpu
from jax.sharding import PartitionSpec as P

limit_value = 7.0
alpha_value = 1.702
norm_eps = 1e-06

MESH = pl.DeviceIdType.MESH
f32 = jnp.float32
bf16 = jnp.bfloat16
scope = jax.named_scope


def activate(gate_pre, up_pre):
    g = jnp.minimum(gate_pre, limit_value)
    u = jnp.clip(up_pre, -limit_value, limit_value)
    return ((u + 1.0) * g / (1.0 + jnp.exp(-alpha_value * g))).astype(bf16)


def partner_of(me, offset, count):
    other = me
    bit = 1
    while bit < count:
        set_bit = (offset // bit) % 2
        other = other + set_bit * bit * (1 - 2 * ((me // bit) % 2))
        bit *= 2
    return other


def split_sources(n_ep):
    near = [d for d in range(1, n_ep) if d & (d - 1) == 0][::-1]
    far = [d for d in range(1, n_ep) if d & (d - 1) != 0][::-1]
    return near, far


def kernel(
    n_ep,
    n_tp,
    q_hbm,
    k_hbm,
    v_hbm,
    x_hbm,
    gain_hbm,
    ids_hbm,
    logits_hbm,
    gate_hbm,
    up_hbm,
    down_hbm,
    mixer_hbm,
    mix_out,
    routed_out,
    q_ref,
    k_ref,
    v_ref,
    x_ref,
    gain_ref,
    ids_ref,
    logits_ref,
    wg,
    wu,
    wd,
    wm,
    xs,
    xr,
    wr,
    kvr,
    pb,
    cr,
    sb,
    rr,
    zb,
    zr,
    at_send,
    at_recv,
    qt_ref,
    kv_ref,
    wt_ref,
    wc,
    acc,
    tot,
    hs,
    ob,
    w_sem,
    in_sem,
    xf_ss,
    xf_rs,
    g_ss,
    g_rs,
    ff_ss,
    ff_rs,
    y_ss,
    y_rs,
    e_ss,
    e_rs,
    cf_rs,
    xn_ss,
    fn_ss,
    xn_rs,
    fn_rs,
    cn_rs,
    rn_rs,
    wt_rs,
    kv_ss,
    kv_rs,
    z_rs,
    a_rs,
    c0_rs,
    r_ss,
    c_ss,
    z_ss,
    a_ss,
    wt_ss,
):
    e = lax.axis_index("ep")
    t = lax.axis_index("tp")
    core = t % 2
    zi = t // 2
    zs = n_tp // 2
    mate = t + 1 - 2 * core
    heads, seqs, seg, hd = qt_ref.shape
    tokens, width = x_ref.shape
    half = tokens // 2
    quarter = tokens // 4
    zp = zi % 2
    zmate = t + 2 - 4 * zp
    slots = wt_ref.shape[1]
    local_experts = wg.shape[0]
    ch = width // n_tp
    pp = seg // n_tp
    near, distances = split_sources(n_ep)
    passes = len(near)
    count = len(distances)
    part = tokens // passes
    group = zs // 2
    everything = slice(None)

    weights = [
        pltpu.make_async_copy(src, dst, w_sem.at[i])
        for i, (src, dst) in enumerate(
            ((gate_hbm, wg), (up_hbm, wu), (down_hbm, wd), (mixer_hbm, wm))
        )
    ]
    inputs = [
        pltpu.make_async_copy(src, dst, in_sem.at[i])
        for i, (src, dst) in enumerate(
            (
                (x_hbm, x_ref),
                (q_hbm, q_ref),
                (k_hbm, k_ref),
                (v_hbm, v_ref),
                (ids_hbm, ids_ref),
                (logits_hbm, logits_ref),
                (gain_hbm, gain_ref),
            )
        )
    ]

    def ep_peer(d):
        return partner_of(e, d, n_ep)

    barrier = pltpu.get_barrier_semaphore()
    for d in range(1, n_ep):
        pl.semaphore_signal(barrier, inc=1, device_id={"ep": ep_peer(d)}, device_id_type=MESH)
    for d in range(1, n_tp):
        pl.semaphore_signal(
            barrier, inc=1, device_id={"tp": (t + d) % n_tp}, device_id_type=MESH
        )
    for copy in inputs:
        copy.start()

    def nth(i):
        return sum(jnp.where(i == n, d, 0) for n, d in enumerate(distances))

    def remote(src, dst, send, recv, axis, to):
        return pltpu.make_async_remote_copy(
            src_ref=src,
            dst_ref=dst,
            send_sem=send,
            recv_sem=recv,
            device_id={axis: to},
            device_id_type=MESH,
        )

    def settle_bytes(ref, sem):
        pltpu.make_async_copy(ref, ref, sem).wait()

    mine = pl.ds(pl.multiple_of(core * half, half), half)
    piece = pl.ds(pl.multiple_of(core * half + zp * quarter, quarter), quarter)

    def span(h):
        return pl.ds(pl.multiple_of(h * part, part), part)

    def own_part(h):
        return pl.ds(pl.multiple_of(h * part + core * (part // 2), part // 2), part // 2)

    def xf_copy(i):
        d = nth(i)
        return remote(xs.at[piece], xr.at[d, piece], xf_ss.at[i], xf_rs.at[i], "ep", ep_peer(d))

    def g_copy(i):
        ref = xr.at[nth(i), piece]
        return remote(ref, ref, g_ss.at[i], g_rs.at[i], "tp", zmate)

    def ff_copy(i):
        ref = xr.at[nth(i), mine]
        return remote(ref, ref, ff_ss.at[i], ff_rs.at[i], "tp", mate)

    def xn_copy(n, h):
        rows = own_part(h)
        return remote(
            xs.at[rows],
            xr.at[near[n], rows],
            xn_ss.at[n],
            xn_rs.at[n, h],
            "ep",
            ep_peer(near[n]),
        )

    def fn_copy(n, h):
        ref = xr.at[near[n], own_part(h)]
        return remote(ref, ref, fn_ss.at[n], fn_rs.at[n, h], "tp", mate)

    def wt_copy(d):
        return remote(
            wt_ref.at[ep_peer(d)], wr.at[d], wt_ss.at[0], wt_rs.at[d - 1], "ep", ep_peer(d)
        )

    def kv_copy(d):
        return remote(
            kv_ref, kvr.at[d], kv_ss.at[d - 1], kv_rs.at[d - 1], "ep", (e + d) % n_ep
        )

    def c_copy(d, c, rows, sem):
        return remote(
            pb.at[d, 1 - core, c, rows], cr.at[d, c, rows], c_ss.at[0], sem, "tp", mate
        )

    def r_copy(n, h, k):
        c = (zi + k) % zs
        return remote(
            sb.at[near[n], c, span(h)],
            rr.at[near[n], c, span(h)],
            r_ss.at[0],
            rn_rs.at[n, h, k - 1],
            "ep",
            ep_peer(near[n]),
        )

    def y_copy(i, k):
        d = nth(i)
        c = (zi + k) % zs
        return remote(sb.at[d, c], rr.at[d, k], y_ss.at[i], y_rs.at[i], "tp", c * 2 + core)

    def e_copy(i):
        d = nth(i)
        return remote(sb.at[d, zi], rr.at[d, 0], e_ss.at[i], e_rs.at[i], "ep", ep_peer(d))

    def z_copy(k, h):
        dz = (zi + k) % zs
        return remote(
            zb.at[dz, span(h)],
            zr.at[k, span(h)],
            z_ss.at[0],
            z_rs.at[0],
            "tp",
            dz * 2 + core,
        )

    def a_copy(d):
        to = (t + d) % n_tp
        return remote(at_send.at[to], at_recv.at[t], a_ss.at[0], a_rs.at[0], "tp", to)

    with scope("xload"):
        for copy in inputs:
            copy.wait()
    for copy in weights:
        copy.start()

    with scope("norm0"):
        values = x_ref[...].astype(f32)
        mean = jnp.mean(values * values, axis=-1, keepdims=True)
        xs[...] = (values * lax.rsqrt(mean + norm_eps) * gain_ref[...]).astype(bf16)

    top = ids_ref.shape[0]
    logits = [logits_ref[k : k + 1] for k in range(top)]
    peak = functools.reduce(jnp.maximum, logits)
    powers = [jnp.exp(value - peak) for value in logits]
    share = 1.0 / functools.reduce(jnp.add, powers)
    slot = lax.broadcasted_iota(jnp.int32, (slots, tokens), 0)
    for g in range(n_ep):
        expert = jnp.where(slot < local_experts, g * local_experts + slot, -1)
        table = jnp.zeros((slots, tokens), f32)
        for k in range(top):
            table = table + jnp.where(ids_ref[k : k + 1] == expert, powers[k] * share, 0.0)
        wt_ref[g] = table

    with scope("barrier"):
        pl.semaphore_wait(barrier, n_ep - 1 + n_tp - 1)
    for d in range(1, n_ep):
        wt_copy(d).start()
    for i in range(count):
        xf_copy(i).start()
    for h in range(passes):
        for n in range(passes):
            xn_copy(n, h).start()

    rows = hd * seqs
    for s in range(seqs):
        pick = (
            (
                lax.broadcasted_iota(jnp.int32, (hd, rows), 1)
                == lax.broadcasted_iota(jnp.int32, (hd, rows), 0) * seqs + s
            )
            .astype(f32)
            .astype(bf16)
        )
        for h in range(heads):
            kv_ref[0, h, s] = jnp.dot(pick, k_ref[h], preferred_element_type=f32).astype(bf16)
            kv_ref[1, h, s] = jnp.dot(pick, v_ref[h], preferred_element_type=f32).astype(bf16)
            query = jnp.dot(pick, q_ref[h], preferred_element_type=f32)
            qt_ref[h, s] = query.T.astype(bf16)

    def up(j, lhs):
        gate_pre = jnp.dot(lhs(), wg[j], preferred_element_type=f32)
        up_pre = jnp.dot(lhs(), wu[j], preferred_element_type=f32)
        hs[j] = activate(gate_pre, up_pre)

    def down(sources, columns, rows, sems):
        size = tokens // len(sources)
        for k in range(1, zs + 1):
            c = (zi + k) % zs
            for p in range(2):
                place = pl.ds(pl.multiple_of((2 * c + p) * ch, ch), ch)
                terms = [
                    jnp.dot(hs[j], wd[j, :, place], preferred_element_type=f32)
                    for j in range(local_experts)
                ]
                for n, d in enumerate(sources):
                    total = None
                    for j in range(local_experts):
                        term = columns[n][:, j : j + 1] * terms[j][n * size : (n + 1) * size]
                        total = term if total is None else total + term
                    pb[d, p, c, rows] = total.astype(bf16)
            if k % group == 0:
                for q in range(k - group + 1, k + 1):
                    for d in sources:
                        c_copy(d, (zi + q) % zs, rows, sems.at[k // group - 1]).start()

    def joined(d, c, rows):
        sb[d, c, rows] = (pb[d, core, c, rows].astype(f32) + cr[d, c, rows].astype(f32)).astype(
            bf16
        )

    def finish_own():
        for b in range(2):
            settle_bytes(cr.at[0, pl.ds(0, group)], c0_rs.at[b])
        for c in range(zs):
            joined(0, c, everything)

    def finish_far(i):
        d = nth(i)
        for b in range(2):
            settle_bytes(cr.at[d, pl.ds(0, group)], cf_rs.at[i, b])
            for k in range(b * group + 1, (b + 1) * group + 1):
                joined(d, (zi + k) % zs, everything)
                if k < zs:
                    y_copy(i, k).start()

    def finish_near(h):
        for b in range(2):
            settle_bytes(cr.at[pl.ds(0, passes), pl.ds(0, group), span(h)], cn_rs.at[h, b])
            for k in range(b * group + 1, (b + 1) * group + 1):
                for n in range(passes):
                    joined(near[n], (zi + k) % zs, span(h))
                    r_copy(n, h, k).start()

    def gathered(i):
        d = nth(i)
        settle_bytes(rr.at[d, pl.ds(0, zs - 1)], y_rs.at[i])
        total = sb[d, zi].astype(f32)
        for k in range(1, zs):
            total = total + rr[d, k].astype(f32)
        sb[d, zi] = total.astype(bf16)
        e_copy(i).start()

    def settle(h):
        for k in range(1, zs + 1):
            c = (zi + k) % zs
            own = sb[0, c, span(h)].astype(f32)
            for n in range(passes):
                r_copy(n, h, k).wait_recv()
                own = own + rr[near[n], c, span(h)].astype(f32)
            if k < zs:
                zb[c, span(h)] = own.astype(bf16)
                z_copy(k, h).start()
            else:
                ob[span(h)] = own

    pairs = heads * seqs
    tall = pairs * seg
    row_id = lax.broadcasted_iota(jnp.int32, (2 * seg, 2 * seg), 0) % seg
    col_id = lax.broadcasted_iota(jnp.int32, (2 * seg, 2 * seg), 1)
    later_mask = ((row_id > col_id) | (col_id >= seg)).astype(f32).astype(bf16)
    scale = hd ** (-0.5)

    def block(kv, diagonal):
        scores = jnp.concatenate(
            [
                jnp.dot(qt_ref[p // seqs, p % seqs], kv[0, p // seqs, p % seqs],
                        preferred_element_type=f32)
                for p in range(pairs)
            ],
            axis=0,
        ) * scale
        log_term = jnp.log(1.0 + jnp.exp(-jnp.abs(scores)))
        keep = -(jnp.maximum(scores, 0.0) + log_term)
        beta = jnp.minimum(scores, 0.0) - log_term
        if diagonal:
            usable = lax.broadcasted_iota(jnp.int32, (tall, seg), 1) < (
                lax.broadcasted_iota(jnp.int32, (tall, seg), 0) % seg
            )
            keep = jnp.where(usable, keep, 0.0)
        high = keep.astype(bf16)
        low = (keep - high.astype(f32)).astype(bf16)
        sums = jnp.dot(
            jnp.concatenate([high, low], axis=1), later_mask, preferred_element_type=f32
        )
        weight = jnp.exp(beta + sums[:, :seg])
        if diagonal:
            weight = jnp.where(usable, weight, 0.0)
        weight = weight.astype(bf16)
        out = jnp.concatenate(
            [
                lax.dot_general(
                    weight[p * seg : (p + 1) * seg],
                    kv[1, p // seqs, p % seqs],
                    (((1,), (1,)), ((), ())),
                    preferred_element_type=f32,
                )
                for p in range(pairs)
            ],
            axis=0,
        )
        return out, sums[:, seg : seg + hd]

    with scope("diag"):
        acc[...], tot[...] = block(kv_ref, True)

    with scope("waitfar"):
        for i in range(count):
            xf_copy(i).wait_recv()
            g_copy(i).start()
    with scope("weights"):
        for copy in weights[:3]:
            copy.wait()
    with scope("up0"):
        for j in range(local_experts):
            up(j, lambda: xs[...])
    with scope("down0"):
        down([0], [wt_ref[e].T], everything, c0_rs)
    for k in range(1, n_ep):

        @pl.when(e + k < n_ep)
        def _():
            kv_copy(k).start()

    def share_near(h):
        with scope("xwait"):
            for n in range(passes):
                xn_copy(n, h).wait_recv()
                fn_copy(n, h).start()

    def share_far(i):
        with scope("gwait"):
            g_copy(i).wait_recv()
            ff_copy(i).start()

    def near_pass(h, middle):
        with scope("fwait"):
            for n in range(passes):
                fn_copy(n, h).wait_recv()

        def lhs():
            return jnp.concatenate([xr[d, span(h)] for d in near], axis=0)

        for j in range(local_experts):
            with scope("up"):
                up(j, lhs)
            if j == 0:
                middle()
        with scope("down"):
            down(near, [wc[n, span(h)] for n in range(passes)], span(h), cn_rs.at[h])

    def far_pass(i, middle):
        d = nth(i)
        with scope("fwait"):
            ff_copy(i).wait_recv()
        for j in range(local_experts):
            with scope("up"):
                up(j, lambda: xr[d])
            if j == 0:
                middle()
        with scope("downfar"):
            wt_copy(d).wait_recv()
            down([d], [wr[d].T], everything, cf_rs.at[i])

    def first_passes(h, carry):
        share_near(h)

        def middle():
            with scope("finish"):

                @pl.when(h > 0)
                def _():
                    finish_near(h - 1)

                @pl.when(h == 0)
                def _():
                    finish_own()

            if distances:

                @pl.when(h == passes - 2)
                def _():
                    share_far(0)

        near_pass(h, middle)
        return carry

    def far_passes(i, carry):
        def middle():
            @pl.when(i == 0)
            def _():
                with scope("finish"):
                    finish_near(passes - 2)

            @pl.when(i > 0)
            def _():
                finish_far(i - 1)

            @pl.when(i < count - 1)
            def _():
                share_far(i + 1)

            @pl.when(i == count - 1)
            def _():
                share_near(passes - 1)

        far_pass(i, middle)
        return carry

    def last_middle():
        with scope("finishfar"):
            if distances:
                finish_far(count - 1)
            else:
                finish_own()

    for n in range(passes):
        wt_copy(near[n]).wait_recv()
        wc[n] = wr[near[n]].T
    lax.fori_loop(0, passes - 1, first_passes, 0)
    lax.fori_loop(0, count, far_passes, 0)
    if not distances:
        share_near(passes - 1)
    near_pass(passes - 1, last_middle)
    with scope("finlast"):
        finish_near(passes - 1)

    def further(d, carry):
        kv_copy(d).wait_recv()
        out, total = block(kvr.at[d], False)
        later = tot[...]
        acc[...] = acc[...] + jnp.exp(later) * out
        tot[...] = later + total
        return carry

    with scope("further"):
        lax.fori_loop(1, e + 1, further, 0)
    with scope("asend"):
        for p in range(pairs):
            h, s = p // seqs, p % seqs
            for c in range(n_tp):
                at_send[c, s * pp : (s + 1) * pp, h * hd : (h + 1) * hd] = acc[
                    p * seg + c * pp : p * seg + (c + 1) * pp
                ].astype(bf16)
        for d in range(1, n_tp):
            a_copy(d).start()
        at_recv[t] = at_send[t]

    for h in range(passes):
        if h == passes - 1:
            with scope("gathered"):
                lax.fori_loop(0, count, lambda i, carry: (gathered(i), carry)[1], 0)
        with scope("settle"):
            settle(h)

    with scope("wmix"):
        weights[3].wait()
    with scope("await"):
        settle_bytes(at_recv.at[pl.ds(0, n_tp - 1)], a_rs.at[0])
    with scope("mix"):
        wide = jnp.concatenate([at_recv[c] for c in range(n_tp)], axis=1)
        mixed = jnp.dot(wide, wm[...], preferred_element_type=f32)
        for s in range(seqs):
            mix_out[s] = mixed[s * pp : (s + 1) * pp].astype(bf16)

    with scope("zfin"):
        total = ob[...]
        settle_bytes(zr.at[pl.ds(0, zs - 1)], z_rs.at[0])
        for k in range(1, zs):
            total = total + zr[k].astype(f32)
        for i, d in enumerate(distances):
            e_copy(i).wait_recv()
            total = total + rr[d, 0].astype(f32)
        routed_out[...] = total.T.astype(bf16)

    with scope("drain"):
        settle_bytes(wt_ref.at[pl.ds(0, n_ep - 1)], wt_ss.at[0])
        for i in range(count):
            xf_copy(i).wait_send()
            g_copy(i).wait_send()
            ff_copy(i).wait_send()
            settle_bytes(sb.at[0, pl.ds(0, zs - 1)], y_ss.at[i])
            e_copy(i).wait_send()
        for n in range(passes):
            settle_bytes(xs.at[mine], xn_ss.at[n])
            settle_bytes(xs.at[mine], fn_ss.at[n])
        settle_bytes(cr, c_ss.at[0])
        settle_bytes(sb.at[pl.ds(0, passes)], r_ss.at[0])
        settle_bytes(zb.at[pl.ds(0, zs - 1)], z_ss.at[0])
        settle_bytes(at_send.at[pl.ds(0, n_tp - 1)], a_ss.at[0])
        for k in range(1, n_ep):

            @pl.when(e + k < n_ep)
            def _():
                kv_copy(k).wait_send()


def hand_over(mixed_ref, routed_ref, mix_out, routed_out, sems):
    copies = [
        pltpu.make_async_copy(src, dst, sems.at[i])
        for i, (src, dst) in enumerate(((mixed_ref, mix_out), (routed_ref, routed_out)))
    ]
    for copy in copies:
        copy.start()
    for copy in copies:
        copy.wait()


def body(
    queries,
    key_vectors,
    value_vectors,
    mixer_weight,
    expert_rows,
    norm_gain,
    route_ids,
    route_logits,
    gate_weight,
    up_weight,
    down_weight,
):
    n_ep, n_tp = lax.axis_size("ep"), lax.axis_size("tp")
    heads, hd, seqs, seg = queries.shape
    tokens, width = expert_rows.shape
    local_experts, _, ff = gate_weight.shape
    zs, ch, pp = n_tp // 2, width // n_tp, seg // n_tp

    top = route_ids.shape[1]
    slots = 8 * -(-local_experts // 8)
    pairs = heads * seqs
    near, distances = split_sources(n_ep)
    passes, count = len(near), max(len(distances), 1)
    kv_shape = (2, heads, seqs, hd, seg)

    def merged(rows):
        return rows.reshape(heads, hd * seqs, seg)

    vmem = pl.BlockSpec(memory_space=pltpu.VMEM)
    anywhere = pl.BlockSpec(memory_space=pltpu.HBM)
    dma = pltpu.SemaphoreType.DMA
    outs = 2 * seqs * pp * width + 2 * ch * tokens
    limit = (60 * 1024 * 1024) - outs - (64 << 10)
    shapes = ((seqs, pp, width), (ch, tokens))
    results = pl.pallas_call(
        functools.partial(kernel, n_ep, n_tp),
        out_shape=tuple(pltpu.VMEM(shape, bf16) for shape in shapes),
        in_specs=[anywhere] * 11,
        out_specs=(vmem, vmem),
        scratch_shapes=[
            pltpu.VMEM((heads, hd * seqs, seg), bf16),
            pltpu.VMEM((heads, hd * seqs, seg), bf16),
            pltpu.VMEM((heads, hd * seqs, seg), bf16),
            pltpu.VMEM((tokens, width), bf16),
            pltpu.VMEM((1, width), f32),
            pltpu.VMEM((top, tokens), jnp.int32),
            pltpu.VMEM((top, tokens), f32),
            pltpu.VMEM(gate_weight.shape, bf16),
            pltpu.VMEM(up_weight.shape, bf16),
            pltpu.VMEM(down_weight.shape, bf16),
            pltpu.VMEM(mixer_weight.shape, bf16),
            pltpu.VMEM((tokens, width), bf16),
            pltpu.VMEM((n_ep, tokens, width), bf16),
            pltpu.VMEM((n_ep, slots, tokens), f32),
            pltpu.VMEM((n_ep,) + kv_shape, bf16),
            pltpu.VMEM((n_ep, 2, zs, tokens, ch), bf16),
            pltpu.VMEM((n_ep, zs, tokens, ch), bf16),
            pltpu.VMEM((n_ep, zs, tokens, ch), bf16),
            pltpu.VMEM((n_ep, zs, tokens, ch), bf16),
            pltpu.VMEM((zs, tokens, ch), bf16),
            pltpu.VMEM((zs, tokens, ch), bf16),
            pltpu.VMEM((n_tp, seqs * pp, heads * hd), bf16),
            pltpu.VMEM((n_tp, seqs * pp, heads * hd), bf16),
            pltpu.VMEM((heads, seqs, seg, hd), bf16),
            pltpu.VMEM(kv_shape, bf16),
            pltpu.VMEM((n_ep, slots, tokens), f32),
            pltpu.VMEM((passes, tokens, slots), f32),
            pltpu.VMEM((pairs * seg, hd), f32),
            pltpu.VMEM((pairs * seg, hd), f32),
            pltpu.VMEM((local_experts, tokens, ff), bf16),
            pltpu.VMEM((tokens, ch), f32),
            dma((4,)),
            dma((7,)),
        ]
        + [dma((count,))] * 10
        + [dma((count, 2))]
        + [dma((passes,))] * 2
        + [dma((passes, passes))] * 2
        + [dma((passes, 2)), dma((passes, passes, zs))]
        + [dma((n_ep - 1,))] * 3
        + [dma((1,))] * 2
        + [dma((2,))]
        + [dma((1,))] * 5,
        compiler_params=pltpu.CompilerParams(
            collective_id=0, has_side_effects=True, vmem_limit_bytes=limit
        ),
    )(
        merged(queries),
        merged(key_vectors),
        merged(value_vectors),
        expert_rows,
        norm_gain[None, :],
        route_ids.T,
        route_logits.T,
        gate_weight,
        up_weight,
        down_weight,
        mixer_weight,
    )
    return pl.pallas_call(
        hand_over,
        out_shape=tuple(jax.ShapeDtypeStruct(shape, bf16) for shape in shapes),
        in_specs=[vmem] * 2,
        out_specs=(anywhere, anywhere),
        scratch_shapes=[dma((2,))],
        compiler_params=pltpu.CompilerParams(vmem_limit_bytes=1 << 20),
    )(*results)


def solution(mesh):
    in_specs = (
        P("tp", None, None, "ep"),
        P("tp", None, None, "ep"),
        P("tp", None, None, "ep"),
        P(),
        P("ep", None),
        P(),
        P("ep", None),
        P("ep", None),
        P("ep", None, "tp"),
        P("ep", None, "tp"),
        P("ep", "tp", None),
    )
    out_specs = (P(None, ("ep", "tp"), None), P("tp", "ep"))
    return jax.shard_map(body, mesh=mesh, in_specs=in_specs, out_specs=out_specs, check_vma=False)
```

profile of v0, /device:TPU:0, one launch (start us, length us, event | category | flops | bytes accessed | tf_op | source)
XLA Modules:
  0.0 38.1 jit_solution(11514813214455852335)
XLA Ops:
  0.6 36.8 %shard_map.122 = (bf16[2,16,2048]{2,1,0:T(8,128)(2,1)S(1)}, bf16[256,128]{1,0:T(8,128)(2,1)S(1)}) custom-call(bf16[2,128,128]{2,1,0:T(8,128)(2,1)} %bitcast.6, bf16[2,128,128]{2,1,0:T(8,128)(2,1)} %bitcast.7, bf16[2,128,128]{2,1,0:T(8,128)(2,1)} %bitcast.8, bf16[128,2048]{1,0:T(8,128)(2,1)} %x_hbm.1, f32[1,2048]{1,0:T(1,128)} %bitcast.9, s32[2,128]{1,0:T(2,128)} %bitcast.10, ...), custom_call_target="tpu_custom_call" | custom-call | tf_op jit(solution)/shard_map/pallas_call | solution.py:692
  37.4 0.7 %shard_map.123 = (bf16[2,16,2048]{2,1,0:T(8,128)(2,1)}, bf16[256,128]{1,0:T(8,128)(2,1)}) custom-call(bf16[2,16,2048]{2,1,0:T(8,128)(2,1)S(1)} %get-tuple-element.4.mixed_ref, bf16[256,128]{1,0:T(8,128)(2,1)S(1)} %get-tuple-element.5.routed_ref), custom_call_target="tpu_custom_call" | custom-call | tf_op jit(solution)/shard_map/pallas_call | solution.py:757
where the time goes:
time: 38.3 us; the launch traced here: 38.1 us
  Pallas kernels  37.5 us (98%)
  between operations  0.64 us (2%)
    pallas_call x1, Pallas kernels, body(): pl.pallas_call(functools.partial(kernel, n_ep, n_tp), out_shape=tuple((pl...  36.8 us

commit v1 on v0

--- a/solution.py
+++ b/solution.py
@@ -17,10 +17,11 @@
 scope = jax.named_scope
 
 
-def activate(gate_pre, up_pre):
+def activate(gate_pre, up_pre, weight):
     g = jnp.minimum(gate_pre, limit_value)
     u = jnp.clip(up_pre, -limit_value, limit_value)
-    return ((u + 1.0) * g / (1.0 + jnp.exp(-alpha_value * g))).astype(bf16)
+    sigmoid2 = 1.0 + jnp.tanh((0.5 * alpha_value) * g)
+    return ((u + 1.0) * (g * (0.5 * weight)) * sigmoid2).astype(bf16)
 
 
 def partner_of(me, offset, count):
@@ -86,6 +87,7 @@
     tot,
     hs,
     ob,
+    ex,
     w_sem,
     in_sem,
     xf_ss,
@@ -98,7 +100,9 @@
     y_rs,
     e_ss,
     e_rs,
+    d_ss,
     cf_rs,
+    d_rs,
     xn_ss,
     fn_ss,
     xn_rs,
@@ -137,7 +141,7 @@
     passes = len(near)
     count = len(distances)
     part = tokens // passes
-    group = zs // 2
+    upper, lower = pl.ds(0, half), pl.ds(half, half)
     everything = slice(None)
 
     weights = [
@@ -174,6 +178,14 @@
     for copy in inputs:
         copy.start()
 
+    orders = [
+        sorted((c for c in range(zs) if c != z), key=lambda c: -abs(c - z)) + [z]
+        for z in range(zs)
+    ]
+
+    def chunk(k):
+        return sum(jnp.where(zi == z, order[k - 1], 0) for z, order in enumerate(orders))
+
     def nth(i):
         return sum(jnp.where(i == n, d, 0) for n, d in enumerate(distances))
 
@@ -242,7 +254,7 @@
         )
 
     def r_copy(n, h, k):
-        c = (zi + k) % zs
+        c = chunk(k)
         return remote(
             sb.at[near[n], c, span(h)],
             rr.at[near[n], c, span(h)],
@@ -254,18 +266,39 @@
 
     def y_copy(i, k):
         d = nth(i)
-        c = (zi + k) % zs
-        return remote(sb.at[d, c], rr.at[d, k], y_ss.at[i], y_rs.at[i], "tp", c * 2 + core)
+        c = chunk(k)
+        return remote(
+            sb.at[d, c, upper],
+            rr.at[d, zi, upper],
+            y_ss.at[i],
+            y_rs.at[i],
+            "tp",
+            c * 2 + core,
+        )
 
     def e_copy(i):
         d = nth(i)
-        return remote(sb.at[d, zi], rr.at[d, 0], e_ss.at[i], e_rs.at[i], "ep", ep_peer(d))
+        return remote(
+            sb.at[d, zi, upper], ex.at[i], e_ss.at[i], e_rs.at[i], "ep", ep_peer(d)
+        )
+
+    def d_copy(i, k):
+        d = nth(i)
+        c = chunk(k)
+        return remote(
+            sb.at[d, c, lower],
+            rr.at[d, c, lower],
+            d_ss.at[i],
+            d_rs.at[i, k - 1],
+            "ep",
+            ep_peer(d),
+        )
 
     def z_copy(k, h):
-        dz = (zi + k) % zs
+        dz = chunk(k)
         return remote(
             zb.at[dz, span(h)],
-            zr.at[k, span(h)],
+            zr.at[zi, span(h)],
             z_ss.at[0],
             z_rs.at[0],
             "tp",
@@ -306,9 +339,8 @@
         wt_copy(d).start()
     for i in range(count):
         xf_copy(i).start()
-    for h in range(passes):
-        for n in range(passes):
-            xn_copy(n, h).start()
+    for n in range(passes):
+        xn_copy(n, 0).start()
 
     rows = hd * seqs
     for s in range(seqs):
@@ -326,31 +358,29 @@
             query = jnp.dot(pick, q_ref[h], preferred_element_type=f32)
             qt_ref[h, s] = query.T.astype(bf16)
 
-    def up(j, lhs):
+    def up(j, lhs, columns):
         gate_pre = jnp.dot(lhs(), wg[j], preferred_element_type=f32)
         up_pre = jnp.dot(lhs(), wu[j], preferred_element_type=f32)
-        hs[j] = activate(gate_pre, up_pre)
-
-    def down(sources, columns, rows, sems):
+        hs[j] = activate(gate_pre, up_pre, columns[:, j : j + 1])
+
+    def down(sources, rows, sem):
         size = tokens // len(sources)
         for k in range(1, zs + 1):
-            c = (zi + k) % zs
+            c = chunk(k)
             for p in range(2):
                 place = pl.ds(pl.multiple_of((2 * c + p) * ch, ch), ch)
-                terms = [
-                    jnp.dot(hs[j], wd[j, :, place], preferred_element_type=f32)
-                    for j in range(local_experts)
-                ]
+                total = functools.reduce(
+                    jnp.add,
+                    [
+                        jnp.dot(hs[j], wd[j, :, place], preferred_element_type=f32)
+                        for j in range(local_experts)
+                    ],
+                ).astype(bf16)
                 for n, d in enumerate(sources):
-                    total = None
-                    for j in range(local_experts):
-                        term = columns[n][:, j : j + 1] * terms[j][n * size : (n + 1) * size]
-                        total = term if total is None else total + term
-                    pb[d, p, c, rows] = total.astype(bf16)
-            if k % group == 0:
-                for q in range(k - group + 1, k + 1):
-                    for d in sources:
-                        c_copy(d, (zi + q) % zs, rows, sems.at[k // group - 1]).start()
+                    pb[d, p, c, rows] = total[n * size : (n + 1) * size]
+        for k in range(1, zs + 1):
+            for d in sources:
+                c_copy(d, chunk(k), rows, sem).start()
 
     def joined(d, c, rows):
         sb[d, c, rows] = (pb[d, core, c, rows].astype(f32) + cr[d, c, rows].astype(f32)).astype(
@@ -358,44 +388,47 @@
         )
 
     def finish_own():
-        for b in range(2):
-            settle_bytes(cr.at[0, pl.ds(0, group)], c0_rs.at[b])
+        settle_bytes(cr.at[0], c0_rs.at[0])
         for c in range(zs):
             joined(0, c, everything)
 
     def finish_far(i):
         d = nth(i)
-        for b in range(2):
-            settle_bytes(cr.at[d, pl.ds(0, group)], cf_rs.at[i, b])
-            for k in range(b * group + 1, (b + 1) * group + 1):
-                joined(d, (zi + k) % zs, everything)
-                if k < zs:
-                    y_copy(i, k).start()
+        settle_bytes(cr.at[d], cf_rs.at[i])
+        for k in range(1, zs + 1):
+            joined(d, chunk(k), everything)
+            d_copy(i, k).start()
+            if k < zs:
+                y_copy(i, k).start()
 
     def finish_near(h):
-        for b in range(2):
-            settle_bytes(cr.at[pl.ds(0, passes), pl.ds(0, group), span(h)], cn_rs.at[h, b])
-            for k in range(b * group + 1, (b + 1) * group + 1):
-                for n in range(passes):
-                    joined(near[n], (zi + k) % zs, span(h))
-                    r_copy(n, h, k).start()
+        settle_bytes(cr.at[pl.ds(0, passes), :, span(h)], cn_rs.at[h])
+        for k in range(1, zs + 1):
+            for n in range(passes):
+                joined(near[n], chunk(k), span(h))
+                r_copy(n, h, k).start()
 
     def gathered(i):
         d = nth(i)
-        settle_bytes(rr.at[d, pl.ds(0, zs - 1)], y_rs.at[i])
-        total = sb[d, zi].astype(f32)
+        settle_bytes(rr.at[d, pl.ds(0, zs - 1), upper], y_rs.at[i])
+        total = sb[d, zi, upper].astype(f32)
         for k in range(1, zs):
-            total = total + rr[d, k].astype(f32)
-        sb[d, zi] = total.astype(bf16)
+            total = total + rr[d, chunk(k), upper].astype(f32)
+        sb[d, zi, upper] = total.astype(bf16)
         e_copy(i).start()
 
     def settle(h):
         for k in range(1, zs + 1):
-            c = (zi + k) % zs
+            c = chunk(k)
             own = sb[0, c, span(h)].astype(f32)
             for n in range(passes):
                 r_copy(n, h, k).wait_recv()
                 own = own + rr[near[n], c, span(h)].astype(f32)
+            if h * part >= half:
+                for i, d in enumerate(distances):
+                    if h * part == half:
+                        d_copy(i, k).wait_recv()
+                    own = own + rr[d, c, span(h)].astype(f32)
             if k < zs:
                 zb[c, span(h)] = own.astype(bf16)
                 z_copy(k, h).start()
@@ -452,24 +485,6 @@
     with scope("diag"):
         acc[...], tot[...] = block(kv_ref, True)
 
-    with scope("waitfar"):
-        for i in range(count):
-            xf_copy(i).wait_recv()
-            g_copy(i).start()
-    with scope("weights"):
-        for copy in weights[:3]:
-            copy.wait()
-    with scope("up0"):
-        for j in range(local_experts):
-            up(j, lambda: xs[...])
-    with scope("down0"):
-        down([0], [wt_ref[e].T], everything, c0_rs)
-    for k in range(1, n_ep):
-
-        @pl.when(e + k < n_ep)
-        def _():
-            kv_copy(k).start()
-
     def share_near(h):
         with scope("xwait"):
             for n in range(passes):
@@ -481,6 +496,31 @@
             g_copy(i).wait_recv()
             ff_copy(i).start()
 
+    with scope("weights"):
+        for copy in weights[:3]:
+            copy.wait()
+    own_columns = wt_ref[e].T
+    with scope("up0"):
+        up(0, lambda: xs[...], own_columns)
+    with scope("waitfar"):
+        for i in range(count):
+            xf_copy(i).wait_recv()
+            g_copy(i).start()
+        for h in range(1, passes):
+            for n in range(passes):
+                xn_copy(n, h).start()
+    with scope("up0"):
+        for j in range(1, local_experts):
+            up(j, lambda: xs[...], own_columns)
+    share_near(0)
+    with scope("down0"):
+        down([0], everything, c0_rs.at[0])
+    for k in range(1, n_ep):
+
+        @pl.when(e + k < n_ep)
+        def _():
+            kv_copy(k).start()
+
     def near_pass(h, middle):
         with scope("fwait"):
             for n in range(passes):
@@ -489,29 +529,33 @@
         def lhs():
             return jnp.concatenate([xr[d, span(h)] for d in near], axis=0)
 
+        columns = jnp.concatenate([wc[n, span(h)] for n in range(passes)], axis=0)
         for j in range(local_experts):
             with scope("up"):
-                up(j, lhs)
+                up(j, lhs, columns)
             if j == 0:
                 middle()
         with scope("down"):
-            down(near, [wc[n, span(h)] for n in range(passes)], span(h), cn_rs.at[h])
+            down(near, span(h), cn_rs.at[h])
 
     def far_pass(i, middle):
         d = nth(i)
         with scope("fwait"):
             ff_copy(i).wait_recv()
+            wt_copy(d).wait_recv()
+        columns = wr[d].T
         for j in range(local_experts):
             with scope("up"):
-                up(j, lambda: xr[d])
+                up(j, lambda: xr[d], columns)
             if j == 0:
                 middle()
         with scope("downfar"):
-            wt_copy(d).wait_recv()
-            down([d], [wr[d].T], everything, cf_rs.at[i])
+            down([d], everything, cf_rs.at[i])
 
     def first_passes(h, carry):
-        share_near(h)
+        @pl.when(h > 0)
+        def _():
+            share_near(h)
 
         def middle():
             with scope("finish"):
@@ -612,13 +656,13 @@
             mix_out[s] = mixed[s * pp : (s + 1) * pp].astype(bf16)
 
     with scope("zfin"):
-        total = ob[...]
         settle_bytes(zr.at[pl.ds(0, zs - 1)], z_rs.at[0])
-        for k in range(1, zs):
-            total = total + zr[k].astype(f32)
         for i, d in enumerate(distances):
             e_copy(i).wait_recv()
-            total = total + rr[d, 0].astype(f32)
+            ob[upper] = ob[upper] + ex[i].astype(f32)
+        total = ob[...]
+        for k in range(1, zs):
+            total = total + zr[chunk(k)].astype(f32)
         routed_out[...] = total.T.astype(bf16)
 
     with scope("drain"):
@@ -627,7 +671,8 @@
             xf_copy(i).wait_send()
             g_copy(i).wait_send()
             ff_copy(i).wait_send()
-            settle_bytes(sb.at[0, pl.ds(0, zs - 1)], y_ss.at[i])
+            settle_bytes(sb.at[0, pl.ds(0, zs - 1), upper], y_ss.at[i])
+            settle_bytes(sb.at[0, :, upper], d_ss.at[i])
             e_copy(i).wait_send()
         for n in range(passes):
             settle_bytes(xs.at[mine], xn_ss.at[n])
@@ -726,18 +771,17 @@
             pltpu.VMEM((pairs * seg, hd), f32),
             pltpu.VMEM((local_experts, tokens, ff), bf16),
             pltpu.VMEM((tokens, ch), f32),
+            pltpu.VMEM((count, tokens // 2, ch), bf16),
             dma((4,)),
             dma((7,)),
         ]
-        + [dma((count,))] * 10
-        + [dma((count, 2))]
+        + [dma((count,))] * 12
+        + [dma((count, zs))]
         + [dma((passes,))] * 2
         + [dma((passes, passes))] * 2
-        + [dma((passes, 2)), dma((passes, passes, zs))]
+        + [dma((passes,)), dma((passes, passes, zs))]
         + [dma((n_ep - 1,))] * 3
-        + [dma((1,))] * 2
-        + [dma((2,))]
-        + [dma((1,))] * 5,
+        + [dma((1,))] * 8,
         compiler_params=pltpu.CompilerParams(
             collective_id=0, has_side_effects=True, vmem_limit_bytes=limit
         ),

time: 38.3 us -> 35.6 us (0.930)
  Pallas kernels: 37.5 us -> 34.8 us
    pallas_call x1, Pallas kernels: 36.8 us -> 34.1 us  [body(): pl.pallas_call(functools.partial(kernel, n_ep, n_tp), out_shape=tuple((pl...]
where the time goes in v1:
time: 35.6 us; the launch traced here: 35.4 us
  Pallas kernels  34.8 us (98%)
  between operations  0.64 us (2%)
    pallas_call x1, Pallas kernels, body(): pl.pallas_call(functools.partial(kernel, n_ep, n_tp), out_shape=tuple((pl...  34.1 us

profile of v1, /device:TPU:0, one launch (start us, length us, event | category | flops | bytes accessed | tf_op | source)
XLA Modules:
  0.0 35.4 jit_solution(16095797698732272758)
XLA Ops:
  0.6 34.1 %shard_map.122 = (bf16[2,16,2048]{2,1,0:T(8,128)(2,1)S(1)}, bf16[256,128]{1,0:T(8,128)(2,1)S(1)}) custom-call(bf16[2,128,128]{2,1,0:T(8,128)(2,1)} %bitcast.6, bf16[2,128,128]{2,1,0:T(8,128)(2,1)} %bitcast.7, bf16[2,128,128]{2,1,0:T(8,128)(2,1)} %bitcast.8, bf16[128,2048]{1,0:T(8,128)(2,1)} %x_hbm.1, f32[1,2048]{1,0:T(1,128)} %bitcast.9, s32[2,128]{1,0:T(2,128)} %bitcast.10, ...), custom_call_target="tpu_custom_call" | custom-call | tf_op jit(solution)/shard_map/pallas_call | solution.py:737
  34.7 0.7 %shard_map.123 = (bf16[2,16,2048]{2,1,0:T(8,128)(2,1)}, bf16[256,128]{1,0:T(8,128)(2,1)}) custom-call(bf16[2,16,2048]{2,1,0:T(8,128)(2,1)S(1)} %get-tuple-element.4.mixed_ref, bf16[256,128]{1,0:T(8,128)(2,1)S(1)} %get-tuple-element.5.routed_ref), custom_call_target="tpu_custom_call" | custom-call | tf_op jit(solution)/shard_map/pallas_call | solution.py:801

commit v2 on v1

--- a/solution.py
+++ b/solution.py
@@ -120,6 +120,7 @@
     z_ss,
     a_ss,
     wt_ss,
+    wave,
 ):
     e = lax.axis_index("ep")
     t = lax.axis_index("tp")
@@ -171,10 +172,46 @@
     barrier = pltpu.get_barrier_semaphore()
     for d in range(1, n_ep):
         pl.semaphore_signal(barrier, inc=1, device_id={"ep": ep_peer(d)}, device_id_type=MESH)
-    for d in range(1, n_tp):
-        pl.semaphore_signal(
-            barrier, inc=1, device_id={"tp": (t + d) % n_tp}, device_id_type=MESH
-        )
+    below, above = zi > 0, zi < zs - 1
+    greeted = n_ep + below.astype(jnp.int32) + above.astype(jnp.int32)
+
+    def signal(sem, to):
+        pl.semaphore_signal(sem, inc=1, device_id={"tp": to}, device_id_type=MESH)
+
+    signal(barrier, mate)
+
+    @pl.when(below)
+    def _():
+        signal(barrier, t - 2)
+
+    @pl.when(above)
+    def _():
+        signal(barrier, t + 2)
+
+    def wave_start():
+        @pl.when(jnp.logical_not(above))
+        def _():
+            signal(wave.at[0], t - 2)
+
+        @pl.when(jnp.logical_not(below))
+        def _():
+            signal(wave.at[1], t + 2)
+
+    def wave_pass(way):
+        @pl.when(below & above)
+        def _():
+            pl.semaphore_wait(wave.at[way], 1)
+            signal(wave.at[way], t + 4 * way - 2)
+
+    def wave_end():
+        @pl.when(jnp.logical_not(below))
+        def _():
+            pl.semaphore_wait(wave.at[0], 1)
+
+        @pl.when(jnp.logical_not(above))
+        def _():
+            pl.semaphore_wait(wave.at[1], 1)
+
     for copy in inputs:
         copy.start()
 
@@ -259,7 +296,7 @@
             sb.at[near[n], c, span(h)],
             rr.at[near[n], c, span(h)],
             r_ss.at[0],
-            rn_rs.at[n, h, k - 1],
+            rn_rs.at[h, k - 1],
             "ep",
             ep_peer(near[n]),
         )
@@ -334,13 +371,14 @@
         wt_ref[g] = table
 
     with scope("barrier"):
-        pl.semaphore_wait(barrier, n_ep - 1 + n_tp - 1)
+        pl.semaphore_wait(barrier, greeted)
     for d in range(1, n_ep):
         wt_copy(d).start()
     for i in range(count):
         xf_copy(i).start()
     for n in range(passes):
         xn_copy(n, 0).start()
+    wave_start()
 
     rows = hd * seqs
     for s in range(seqs):
@@ -421,8 +459,8 @@
         for k in range(1, zs + 1):
             c = chunk(k)
             own = sb[0, c, span(h)].astype(f32)
+            settle_bytes(rr.at[pl.ds(0, passes), c, span(h)], rn_rs.at[h, k - 1])
             for n in range(passes):
-                r_copy(n, h, k).wait_recv()
                 own = own + rr[near[n], c, span(h)].astype(f32)
             if h * part >= half:
                 for i, d in enumerate(distances):
@@ -521,6 +559,9 @@
         def _():
             kv_copy(k).start()
 
+    with scope("wave"):
+        wave_pass(1)
+
     def near_pass(h, middle):
         with scope("fwait"):
             for n in range(passes):
@@ -610,9 +651,13 @@
         wt_copy(near[n]).wait_recv()
         wc[n] = wr[near[n]].T
     lax.fori_loop(0, passes - 1, first_passes, 0)
+    with scope("wave"):
+        wave_pass(0)
     lax.fori_loop(0, count, far_passes, 0)
     if not distances:
         share_near(passes - 1)
+    with scope("wavend"):
+        wave_end()
     near_pass(passes - 1, last_middle)
     with scope("finlast"):
         finish_near(passes - 1)
@@ -779,9 +824,10 @@
         + [dma((count, zs))]
         + [dma((passes,))] * 2
         + [dma((passes, passes))] * 2
-        + [dma((passes,)), dma((passes, passes, zs))]
+        + [dma((passes,)), dma((passes, zs))]
         + [dma((n_ep - 1,))] * 3
-        + [dma((1,))] * 8,
+        + [dma((1,))] * 8
+        + [pltpu.SemaphoreType.REGULAR((2,))],
         compiler_params=pltpu.CompilerParams(
             collective_id=0, has_side_effects=True, vmem_limit_bytes=limit
         ),

time: 35.6 us -> 35.2 us (0.989)
  Pallas kernels: 34.8 us -> 34.2 us
    pallas_call x1, Pallas kernels: 34.1 us -> 33.5 us  [body(): pl.pallas_call(functools.partial(kernel, n_ep, n_tp), out_shape=tuple((pl...]
where the time goes in v2:
time: 35.2 us; the launch traced here: 34.8 us
  Pallas kernels  34.2 us (97%)
  between operations  0.64 us (2%)
    pallas_call x1, Pallas kernels, body(): pl.pallas_call(functools.partial(kernel, n_ep, n_tp), out_shape=tuple((pl...  33.5 us

profile of v2, /device:TPU:0, one launch (start us, length us, event | category | flops | bytes accessed | tf_op | source)
XLA Modules:
  0.0 34.8 jit_solution(10413271947690426896)
XLA Ops:
  0.6 33.5 %shard_map.122 = (bf16[2,16,2048]{2,1,0:T(8,128)(2,1)S(1)}, bf16[256,128]{1,0:T(8,128)(2,1)S(1)}) custom-call(bf16[2,128,128]{2,1,0:T(8,128)(2,1)} %bitcast.6, bf16[2,128,128]{2,1,0:T(8,128)(2,1)} %bitcast.7, bf16[2,128,128]{2,1,0:T(8,128)(2,1)} %bitcast.8, bf16[128,2048]{1,0:T(8,128)(2,1)} %x_hbm.1, f32[1,2048]{1,0:T(1,128)} %bitcast.9, s32[2,128]{1,0:T(2,128)} %bitcast.10, ...), custom_call_target="tpu_custom_call" | custom-call | tf_op jit(solution)/shard_map/pallas_call | solution.py:782
  34.1 0.7 %shard_map.123 = (bf16[2,16,2048]{2,1,0:T(8,128)(2,1)}, bf16[256,128]{1,0:T(8,128)(2,1)}) custom-call(bf16[2,16,2048]{2,1,0:T(8,128)(2,1)S(1)} %get-tuple-element.4.mixed_ref, bf16[256,128]{1,0:T(8,128)(2,1)S(1)} %get-tuple-element.5.routed_ref), custom_call_target="tpu_custom_call" | custom-call | tf_op jit(solution)/shard_map/pallas_call | solution.py:847

commit v3 on v2

--- a/solution.py
+++ b/solution.py
@@ -197,11 +197,14 @@
         def _():
             signal(wave.at[1], t + 2)
 
-    def wave_pass(way):
-        @pl.when(below & above)
-        def _():
-            pl.semaphore_wait(wave.at[way], 1)
-            signal(wave.at[way], t + 4 * way - 2)
+    def wave_pass(first):
+        for way in range(2):
+            turn = (zi < zs // 2) if first == (way == 1) else (zi >= zs // 2)
+
+            @pl.when(below & above & turn)
+            def _():
+                pl.semaphore_wait(wave.at[way], 1)
+                signal(wave.at[way], t + 4 * way - 2)
 
     def wave_end():
         @pl.when(jnp.logical_not(below))
@@ -560,9 +563,9 @@
             kv_copy(k).start()
 
     with scope("wave"):
-        wave_pass(1)
-
-    def near_pass(h, middle):
+        wave_pass(True)
+
+    def near_pass(h, middle, spread=None):
         with scope("fwait"):
             for n in range(passes):
                 fn_copy(n, h).wait_recv()
@@ -574,12 +577,13 @@
         for j in range(local_experts):
             with scope("up"):
                 up(j, lhs, columns)
-            if j == 0:
-                middle()
+            if j == 0 and spread is not None:
+                spread()
+        middle()
         with scope("down"):
             down(near, span(h), cn_rs.at[h])
 
-    def far_pass(i, middle):
+    def far_pass(i, middle, spread):
         d = nth(i)
         with scope("fwait"):
             ff_copy(i).wait_recv()
@@ -589,7 +593,8 @@
             with scope("up"):
                 up(j, lambda: xr[d], columns)
             if j == 0:
-                middle()
+                spread()
+        middle()
         with scope("downfar"):
             down([d], everything, cf_rs.at[i])
 
@@ -609,13 +614,14 @@
                 def _():
                     finish_own()
 
+        def spread():
             if distances:
 
                 @pl.when(h == passes - 2)
                 def _():
                     share_far(0)
 
-        near_pass(h, middle)
+        near_pass(h, middle, spread)
         return carry
 
     def far_passes(i, carry):
@@ -629,6 +635,7 @@
             def _():
                 finish_far(i - 1)
 
+        def spread():
             @pl.when(i < count - 1)
             def _():
                 share_far(i + 1)
@@ -637,7 +644,7 @@
             def _():
                 share_near(passes - 1)
 
-        far_pass(i, middle)
+        far_pass(i, middle, spread)
         return carry
 
     def last_middle():
@@ -646,21 +653,6 @@
                 finish_far(count - 1)
             else:
                 finish_own()
-
-    for n in range(passes):
-        wt_copy(near[n]).wait_recv()
-        wc[n] = wr[near[n]].T
-    lax.fori_loop(0, passes - 1, first_passes, 0)
-    with scope("wave"):
-        wave_pass(0)
-    lax.fori_loop(0, count, far_passes, 0)
-    if not distances:
-        share_near(passes - 1)
-    with scope("wavend"):
-        wave_end()
-    near_pass(passes - 1, last_middle)
-    with scope("finlast"):
-        finish_near(passes - 1)
 
     def further(d, carry):
         kv_copy(d).wait_recv()
@@ -670,18 +662,52 @@
         tot[...] = later + total
         return carry
 
+    def hand_out():
+        with scope("asend"):
+            for p in range(pairs):
+                h, s = p // seqs, p % seqs
+                for c in range(n_tp):
+                    at_send[c, s * pp : (s + 1) * pp, h * hd : (h + 1) * hd] = acc[
+                        p * seg + c * pp : p * seg + (c + 1) * pp
+                    ].astype(bf16)
+            for d in range(1, n_tp):
+                a_copy(d).start()
+            at_recv[t] = at_send[t]
+
+    for n in range(passes):
+        wt_copy(near[n]).wait_recv()
+        wc[n] = wr[near[n]].T
+    lax.fori_loop(0, passes - 1, first_passes, 0)
+    with scope("wave"):
+        wave_pass(False)
+    lax.fori_loop(0, count, far_passes, 0)
+    if not distances:
+        share_near(passes - 1)
+    with scope("wavend"):
+        wave_end()
+    early = n_ep // 2
+
+    @pl.when(e == 0)
+    def _():
+        hand_out()
+
+    near_pass(passes - 1, last_middle)
     with scope("further"):
-        lax.fori_loop(1, e + 1, further, 0)
-    with scope("asend"):
-        for p in range(pairs):
-            h, s = p // seqs, p % seqs
-            for c in range(n_tp):
-                at_send[c, s * pp : (s + 1) * pp, h * hd : (h + 1) * hd] = acc[
-                    p * seg + c * pp : p * seg + (c + 1) * pp
-                ].astype(bf16)
-        for d in range(1, n_tp):
-            a_copy(d).start()
-        at_recv[t] = at_send[t]
+        lax.fori_loop(1, jnp.minimum(e, early) + 1, further, 0)
+
+    @pl.when((e > 0) & (e <= early))
+    def _():
+        hand_out()
+
+    with scope("finlast"):
+        finish_near(passes - 1)
+    with scope("further"):
+        lax.fori_loop(early + 1, e + 1, further, 0)
+
+    @pl.when(e > early)
+    def _():
+        hand_out()
+
 
     for h in range(passes):
         if h == passes - 1:

time: 35.2 us -> 34.6 us (0.983)
  Pallas kernels: 34.2 us -> 33.7 us
    pallas_call x1, Pallas kernels: 33.5 us -> 33 us  [body(): pl.pallas_call(functools.partial(kernel, n_ep, n_tp), out_shape=tuple((pl...]
where the time goes in v3:
time: 34.6 us; the launch traced here: 34.4 us
  Pallas kernels  33.7 us (97%)
  between operations  0.64 us (2%)
    pallas_call x1, Pallas kernels, body(): pl.pallas_call(functools.partial(kernel, n_ep, n_tp), out_shape=tuple((pl...  33 us
    pallas_call x1, Pallas kernels, body(): pl.pallas_call(hand_over, out_shape=tuple((jax.ShapeDtypeStruct(shape, bf...  0.69 us

profile of v3, /device:TPU:0, one launch (start us, length us, event | category | flops | bytes accessed | tf_op | source)
XLA Modules:
  0.0 34.4 jit_solution(2134507704371250432)
XLA Ops:
  0.6 33.0 %shard_map.122 = (bf16[2,16,2048]{2,1,0:T(8,128)(2,1)S(1)}, bf16[256,128]{1,0:T(8,128)(2,1)S(1)}) custom-call(bf16[2,128,128]{2,1,0:T(8,128)(2,1)} %bitcast.6, bf16[2,128,128]{2,1,0:T(8,128)(2,1)} %bitcast.7, bf16[2,128,128]{2,1,0:T(8,128)(2,1)} %bitcast.8, bf16[128,2048]{1,0:T(8,128)(2,1)} %x_hbm.1, f32[1,2048]{1,0:T(1,128)} %bitcast.9, s32[2,128]{1,0:T(2,128)} %bitcast.10, ...), custom_call_target="tpu_custom_call" | custom-call | tf_op jit(solution)/shard_map/pallas_call | solution.py:808
  33.7 0.7 %shard_map.123 = (bf16[2,16,2048]{2,1,0:T(8,128)(2,1)}, bf16[256,128]{1,0:T(8,128)(2,1)}) custom-call(bf16[2,16,2048]{2,1,0:T(8,128)(2,1)S(1)} %get-tuple-element.4.mixed_ref, bf16[256,128]{1,0:T(8,128)(2,1)S(1)} %get-tuple-element.5.routed_ref), custom_call_target="tpu_custom_call" | custom-call | tf_op jit(solution)/shard_map/pallas_call | solution.py:873

commit v4 on v3

--- a/solution.py
+++ b/solution.py
@@ -556,12 +556,6 @@
     share_near(0)
     with scope("down0"):
         down([0], everything, c0_rs.at[0])
-    for k in range(1, n_ep):
-
-        @pl.when(e + k < n_ep)
-        def _():
-            kv_copy(k).start()
-
     with scope("wave"):
         wave_pass(True)
 
@@ -598,6 +592,16 @@
         with scope("downfar"):
             down([d], everything, cf_rs.at[i])
 
+    def send_kv(later):
+        for k in range(1, n_ep):
+            held = (e % 4 == 0) & (k % 4 < 3)
+
+            @pl.when((e + k < n_ep) & (held == later))
+            def _():
+                kv_copy(k).start()
+
+    send_kv(False)
+
     def first_passes(h, carry):
         @pl.when(h > 0)
         def _():
@@ -620,6 +624,10 @@
                 @pl.when(h == passes - 2)
                 def _():
                     share_far(0)
+
+            @pl.when(h == 0)
+            def _():
+                send_kv(True)
 
         near_pass(h, middle, spread)
         return carry

time: 34.6 us -> 34.3 us (level)
  no operation moved by 1% of the time
where the time goes in v4:
time: 34.3 us; the launch traced here: 34.1 us
  Pallas kernels  33.5 us (98%)
  between operations  0.64 us (2%)
    pallas_call x1, Pallas kernels, body(): pl.pallas_call(functools.partial(kernel, n_ep, n_tp), out_shape=tuple((pl...  32.8 us
    pallas_call x1, Pallas kernels, body(): pl.pallas_call(hand_over, out_shape=tuple((jax.ShapeDtypeStruct(shape, bf...  0.69 us

profile of v4, /device:TPU:0, one launch (start us, length us, event | category | flops | bytes accessed | tf_op | source)
XLA Modules:
  0.0 34.1 jit_solution(13764308616317406503)
XLA Ops:
  0.6 32.8 %shard_map.122 = (bf16[2,16,2048]{2,1,0:T(8,128)(2,1)S(1)}, bf16[256,128]{1,0:T(8,128)(2,1)S(1)}) custom-call(bf16[2,128,128]{2,1,0:T(8,128)(2,1)} %bitcast.6, bf16[2,128,128]{2,1,0:T(8,128)(2,1)} %bitcast.7, bf16[2,128,128]{2,1,0:T(8,128)(2,1)} %bitcast.8, bf16[128,2048]{1,0:T(8,128)(2,1)} %x_hbm.1, f32[1,2048]{1,0:T(1,128)} %bitcast.9, s32[2,128]{1,0:T(2,128)} %bitcast.10, ...), custom_call_target="tpu_custom_call" | custom-call | tf_op jit(solution)/shard_map/pallas_call | solution.py:816
  33.4 0.7 %shard_map.123 = (bf16[2,16,2048]{2,1,0:T(8,128)(2,1)}, bf16[256,128]{1,0:T(8,128)(2,1)}) custom-call(bf16[2,16,2048]{2,1,0:T(8,128)(2,1)S(1)} %get-tuple-element.4.mixed_ref, bf16[256,128]{1,0:T(8,128)(2,1)S(1)} %get-tuple-element.5.routed_ref), custom_call_target="tpu_custom_call" | custom-call | tf_op jit(solution)/shard_map/pallas_call | solution.py:881
